TPU v7x, 32 devices: a whole 2x2x4 slice. The times are simulated.
32 devices in a mesh: ep: 16 (over z, y, x), tp: 2 (over core).
Axes of the slice: x: 2, y: 2, z: 4, core: 2. Of those that a mesh axis runs over, the one named last changes fastest.
Arguments:
- tokens: bfloat16 [512, 2048], P('ep'), may hold values from -6 to 6
- mix_gain: float32 [2048], replicated, may hold values from 0.1 to 1.9
- w_query: bfloat16 [2048, 512], P('ep', 'tp'), may hold values from -0.125 to 0.125
- w_key: bfloat16 [2048, 512], P('ep', 'tp'), may hold values from -0.125 to 0.125
- w_value: bfloat16 [2048, 512], P('ep', 'tp'), may hold values from -0.125 to 0.125
- w_outgate: bfloat16 [2048, 512], P('ep', 'tp'), may hold values from -0.125 to 0.125
- w_igate: bfloat16 [2048, 8], P('ep', 'tp'), may hold values from -0.125 to 0.125
- w_fgate: bfloat16 [2048, 8], P('ep', 'tp'), may hold values from -0.125 to 0.125
- igate_bias: float32 [8], P('tp'), may hold values from -2 to 1
- fgate_bias: float32 [8], P('tp'), may hold values from 0 to 4
- head_gain: float32 [512], P('tp'), may hold values from 0.1 to 1.9
- w_out: bfloat16 [512, 2048], P('tp', 'ep'), may hold values from -0.25 to 0.25
- state_matrix: float32 [512, 8, 64, 64], P('ep', 'tp'), may hold values from -2.4 to 2.4
- state_norm: float32 [512, 8, 64], P('ep', 'tp'), may hold values from -2.4 to 2.4
- state_max: float32 [512, 8], P('ep', 'tp'), may hold values from -4 to 4
- ffn_gain: float32 [2048], replicated, may hold values from 0.1 to 1.9
- w_expert_gate: bfloat16 [16, 2048, 1408], P('ep', None, 'tp'), may hold values from -0.125 to 0.125
- w_expert_up: bfloat16 [16, 2048, 1408], P('ep', None, 'tp'), may hold values from -0.125 to 0.125
- w_expert_down: bfloat16 [16, 1408, 2048], P('ep', 'tp'), may hold values from -0.15625 to 0.15625
- routes: int32 [512, 3], P('ep'), may hold values from 0 to 15, all different within a row; in each aligned block of 32 rows (0 to 31, 32 to 63, ...) at most 12 rows name the same one
- route_weights: float32 [512, 3], P('ep'), may hold values from 0.2 to 1
Outputs:
- mixed: bfloat16 [512, 2048], P('ep')
- new_matrix: float32 [512, 8, 64, 64], P('ep', 'tp')
- new_norm: float32 [512, 8, 64], P('ep', 'tp')
- new_max: float32 [512, 8], P('ep', 'tp')
Inputs may be any that keep to these rules, and one draw needn't show every extreme that they name: `routes`: each row names 3 different experts. Among the rows of one device, no expert is named by more than 12 rows, a bound that some block reaches.
All inputs are finite; a program needn't handle non-finite values.
Results may differ from a plain program's by a relative error of at most 0.017.
Values may be sent and summed in bfloat16 or wider, within the bound.
No kernel may reach another device: no remote copies, remote signals or barrier semaphores. Data moves between devices by JAX's collectives and lax.ppermute only.
A program may use at most 128 MiB of HBM per device.

v0:
```python
import jax
import jax.numpy as jnp
from jax import lax
from jax.sharding import PartitionSpec as P


def rms_scale(values_in, gain_vec):
    widened = values_in.astype(jnp.float32)
    return (
        widened * lax.rsqrt(jnp.mean(widened * widened, axis=-1, keepdims=True) + 1e-06) * gain_vec
    )


def memory_cell(
    query,
    key_row,
    value_row,
    outgate,
    input_pre,
    forget_pre,
    head_gain,
    state_matrix,
    state_norm,
    state_max,
):
    seq_rows, head_count = input_pre.shape
    head_size = query.shape[1] // head_count
    query_heads = query.astype(jnp.float32).reshape(seq_rows, head_count, head_size)
    key_heads = key_row.astype(jnp.float32).reshape(
        seq_rows, head_count, head_size
    ) * head_size ** (-0.5)
    value_heads = value_row.astype(jnp.float32).reshape(seq_rows, head_count, head_size)
    log_forget = jax.nn.log_sigmoid(forget_pre)
    new_max = jnp.maximum(log_forget + state_max, input_pre)
    keep_old = jnp.exp(log_forget + state_max - new_max)
    keep_new = jnp.exp(input_pre - new_max)
    new_matrix = (
        keep_old[:, :, None, None] * state_matrix
        + keep_new[:, :, None, None] * value_heads[:, :, :, None] * key_heads[:, :, None, :]
    )
    new_norm = keep_old[:, :, None] * state_norm + keep_new[:, :, None] * key_heads
    numerator = jnp.einsum(
        "bhvd,bhd->bhv", new_matrix, query_heads, precision=lax.Precision.HIGHEST
    )
    denominator = jnp.sum(new_norm * query_heads, axis=-1)
    cell_read = numerator / jnp.maximum(jnp.abs(denominator), jnp.exp(-new_max))[:, :, None]
    centered = cell_read - jnp.mean(cell_read, axis=-1, keepdims=True)
    variance = jnp.mean(centered * centered, axis=-1, keepdims=True)
    scaled_cell = (centered * lax.rsqrt(variance + 1e-06)).reshape(seq_rows, head_count * head_size)
    cell_out = (scaled_cell * head_gain * jax.nn.sigmoid(outgate.astype(jnp.float32))).astype(
        jnp.bfloat16
    )
    return (cell_out, new_matrix, new_norm, new_max)


def body(
    tokens,
    mix_gain,
    w_query,
    w_key,
    w_value,
    w_outgate,
    w_igate,
    w_fgate,
    igate_bias,
    fgate_bias,
    head_gain,
    w_out,
    state_matrix,
    state_norm,
    state_max,
    ffn_gain,
    w_expert_gate,
    w_expert_up,
    w_expert_down,
    routes,
    route_weights,
):
    seq_rows, width = tokens.shape
    normed = rms_scale(tokens, mix_gain).astype(jnp.bfloat16)
    weight_list = (w_query, w_key, w_value, w_outgate, w_igate, w_fgate)
    spread = lax.all_to_all(normed, "ep", split_axis=1, concat_axis=0, tiled=True)
    joined = jnp.concatenate(weight_list, axis=1)
    summed = lax.psum_scatter(
        jnp.dot(spread, joined, preferred_element_type=jnp.float32),
        "ep",
        scatter_dimension=0,
        tiled=True,
    )
    bounds = [0]
    for weight in weight_list:
        bounds.append(bounds[-1] + weight.shape[1])
    projected = tuple(
        (summed[:, bounds[index] : bounds[index + 1]] for index in range(len(weight_list)))
    )
    query = projected[0].astype(jnp.bfloat16)
    key_row = projected[1].astype(jnp.bfloat16)
    value_row = projected[2].astype(jnp.bfloat16)
    outgate = projected[3].astype(jnp.bfloat16)
    input_pre = projected[4] + igate_bias
    forget_pre = projected[5] + fgate_bias
    cell_out, new_matrix, new_norm, new_max = memory_cell(
        query,
        key_row,
        value_row,
        outgate,
        input_pre,
        forget_pre,
        head_gain,
        state_matrix,
        state_norm,
        state_max,
    )
    partial_out = jnp.dot(
        cell_out,
        lax.all_gather(w_out, "ep", axis=1, tiled=True),
        preferred_element_type=jnp.float32,
    )
    attended = lax.psum(partial_out.astype(jnp.bfloat16), "tp").astype(jnp.float32)
    resid = (tokens.astype(jnp.float32) + attended).astype(jnp.bfloat16)
    normed_two = rms_scale(resid, ffn_gain).astype(jnp.bfloat16)
    ep_count = lax.axis_size("ep")
    local_experts = w_expert_gate.shape[0]
    expert_total = local_experts * ep_count
    top_count = routes.shape[1]
    capacity = max(2, 2 * seq_rows * top_count // expert_total)
    flat_routes = routes.reshape(-1)
    onehot = (flat_routes[:, None] == jnp.arange(expert_total, dtype=jnp.int32)[None, :]).astype(
        jnp.int32
    )
    earlier = jnp.cumsum(onehot, axis=0, dtype=jnp.int32) - onehot
    slots = jnp.sum(onehot * earlier, axis=1, dtype=jnp.int32)
    targets = flat_routes * capacity + slots
    dispatch = (
        targets[:, None] == jnp.arange(expert_total * capacity, dtype=jnp.int32)[None, :]
    ).astype(jnp.bfloat16)
    route_rows = jnp.repeat(normed_two, top_count, axis=0)
    outgoing = jnp.einsum(
        "rs,rd->sd", dispatch, route_rows, preferred_element_type=jnp.float32
    ).astype(jnp.bfloat16)
    outgoing = outgoing.reshape(expert_total, capacity, width)
    received = lax.all_to_all(outgoing, "ep", split_axis=0, concat_axis=0, tiled=True)
    slot_count = received.shape[1]
    regrouped = received.reshape(ep_count, local_experts, slot_count, width)
    gate_pre = jnp.einsum(
        "nxcd,xdf->nxcf", regrouped, w_expert_gate, preferred_element_type=jnp.float32
    )
    up_pre = jnp.einsum(
        "nxcd,xdf->nxcf", regrouped, w_expert_up, preferred_element_type=jnp.float32
    )
    hidden = (jax.nn.silu(gate_pre) * up_pre).astype(jnp.bfloat16)
    partial_down = jnp.einsum(
        "nxcf,xfd->nxcd", hidden, w_expert_down, preferred_element_type=jnp.float32
    )
    expert_sum = lax.psum(partial_down.astype(jnp.bfloat16), "tp")
    finished = expert_sum.reshape(ep_count * local_experts, slot_count, width)
    returned = lax.all_to_all(finished, "ep", split_axis=0, concat_axis=0, tiled=True)
    picked = jnp.dot(
        dispatch,
        returned.reshape(expert_total * capacity, width),
        preferred_element_type=jnp.float32,
    )
    weighted = jnp.sum(
        picked.reshape(seq_rows, top_count, width) * route_weights[:, :, None], axis=1
    )
    mixed = (resid.astype(jnp.float32) + weighted).astype(jnp.bfloat16)
    return (mixed, new_matrix, new_norm, new_max)


def solution(mesh):
    placed = (
        P("ep", None),
        P(),
        P("ep", "tp"),
        P("ep", "tp"),
        P("ep", "tp"),
        P("ep", "tp"),
        P("ep", "tp"),
        P("ep", "tp"),
        P("tp"),
        P("tp"),
        P("tp"),
        P("tp", "ep"),
        P("ep", "tp", None, None),
        P("ep", "tp", None),
        P("ep", "tp"),
        P(),
        P("ep", None, "tp"),
        P("ep", None, "tp"),
        P("ep", "tp", None),
        P("ep", None),
        P("ep", None),
    )
    return jax.shard_map(
        body,
        mesh=mesh,
        in_specs=placed,
        out_specs=(P("ep", None), P("ep", "tp", None, None), P("ep", "tp", None), P("ep", "tp")),
        check_vma=False,
    )
```

profile of v0, /device:TPU:8, one launch (start us, length us, event | category | flops | bytes accessed | tf_op | source)
XLA Modules:
  0.0 342.0 jit_solution(8380659892496630698)
XLA Ops:
  7.2 1.2 fusion.36
  8.4 1.7 copy_bitcast_fusion
  10.1 7.2 %all-to-all-start = ((bf16[32,16,128]{2,0,1:T(8,128)(2,1)}), bf16[32,16,128]{2,0,1:T(8,128)(2,1)S(1)}, u32[]{:S(2)}, u32[]{:S(2)}) async-start(bf16[32,16,128]{2,0,1:T(8,128)(2,1)} %copy_bitcast_fusion), calls=%async_computation | async-start | bytes 262144 | tf_op jit(solution)/shard_map/all_to_all | solution.py:82
  17.3 0.8 copy.58
  19.0 1.1 concatenate.3
  20.0 3.9 %all-to-all-done = bf16[32,16,128]{2,0,1:T(8,128)(2,1)S(1)} async-done(((bf16[32,16,128]{2,0,1:T(8,128)(2,1)}), bf16[32,16,128]{2,0,1:T(8,128)(2,1)S(1)}, u32[]{:S(2)}, u32[]{:S(2)}) %all-to-all-start) | async-done | bytes 131104 | tf_op jit(solution)/shard_map/all_to_all | solution.py:82
  23.9 1.9 fusion.62
  27.3 125.7 %reduce-scatter.2.cloned.1.call-done = f32[32,1032]{1,0:T(8,128)} async-done(((f32[512,1032]{1,0:T(8,128)}), f32[32,1032]{1,0:T(8,128)}) %reduce-scatter.2.cloned.1.call-update) | async-done | bytes 132112 | tf_op jit(solution)/shard_map/reduce_scatter | solution.py:84
  153.0 0.9 convert.9
  154.4 0.9 broadcast_multiply_fusion.3
  155.3 0.8 subtract_exponential_fusion.1
  156.9 3.8 %multiply_add_fusion = f32[32,4,64,64]{3,2,1,0:T(8,128)S(1)} fusion(f32[32,4,64,64]{3,2,1,0:T(8,128)} %param.33, f32[32,4,64]{2,1,0:T(4,128)S(1)} %get-tuple-element.30, f32[32,4,64]{2,1,0:T(4,128)S(1)} %get-tuple-element.31, f32[32,4]{1,0:T(8,128)S(1)} %subtract_exponential_fusion.1), kind=kLoop, calls=%fused_computation | loop fusion | flops 1572864 | bytes 4260352 | tf_op jit(solution)/shard_map/add | solution.py:38
  160.7 2.0 copy-done.1
  162.7 3.4 fusion.63
  166.7 39.0 %all-gather.2.cloned.1.call-done = bf16[256,2048]{1,0:T(8,128)(2,1)} async-done(((bf16[256,128]{1,0:T(8,128)(2,1)}), bf16[256,2048]{1,0:T(8,128)(2,1)}) %all-gather.2.cloned.1.call-update) | async-done | bytes 1048592 | tf_op jit(solution)/shard_map/all_gather | solution.py:116
  205.7 2.2 convolution_convert_fusion.1
  208.4 18.1 %all-reduce.3.cloned.1.call-done = bf16[32,2048]{1,0:T(8,128)(2,1)} async-done(((bf16[32,2048]{1,0:T(8,128)(2,1)}), bf16[32,2048]{1,0:T(8,128)(2,1)}) %all-reduce.3.cloned.1.call-update) | async-done | bytes 131088 | tf_op jit(solution)/shard_map/psum | solution.py:119
  226.5 1.1 fusion.40
  227.6 1.0 fusion.42
  228.8 1.1 reshape.153
  229.9 2.4 convolution_convert_fusion
  232.3 2.1 reshape.154
  234.4 33.1 %all_to_all.29 = bf16[16,12,2048]{2,1,0:T(8,128)(2,1)S(1)} all-to-all(bf16[16,12,2048]{2,1,0:T(8,128)(2,1)} %reshape.154), channel_id=1, replica_groups=mesh['ep'=16,'tp'=2] {'ep'}, dimensions={0} | all-to-all | bytes 1572864 | tf_op jit(solution)/shard_map/all_to_all | solution.py:142
  267.5 1.0 copy-done.4
  268.5 3.8 %fusion.9 = f32[16,1,12,704]{3,0,2,1:T(8,128)} fusion(bf16[1,2048,704]{1,2,0:T(8,128)(2,1)} %param.37, bf16[16,12,2048]{2,1,0:T(8,128)(2,1)S(1)} %all_to_all.29), kind=kOutput, calls=%fused_computation.11 | convolution fusion | flops 553648128 | bytes 4210688 | tf_op jit(solution)/shard_map/nxcd,xdf->nxcf/dot_general | solution.py:145
  272.3 5.2 %fusion.6 = bf16[16,12,2048]{2,0,1:T(8,128)(2,1)} fusion(bf16[1,704,2048]{2,1,0:T(8,128)(2,1)S(1)} %copy-done, bf16[1,2048,704]{1,2,0:T(8,128)(2,1)} %param.38, f32[16,1,12,704]{3,0,2,1:T(8,128)} %fusion.9, bf16[16,12,2048]{2,1,0:T(8,128)(2,1)} %copy-done.4), kind=kOutput, calls=%fused_computation.7 | convolution fusion | flops 1108500480 | bytes 7880704 | tf_op jit(solution)/shard_map/nxcf,xfd->nxcd/dot_general | solution.py:152
  277.6 17.9 %all-reduce.5.cloned.1.call-done = bf16[16,12,2048]{2,0,1:T(8,128)(2,1)} async-done(((bf16[16,12,2048]{2,0,1:T(8,128)(2,1)}), bf16[16,12,2048]{2,0,1:T(8,128)(2,1)}) %all-reduce.5.cloned.1.call-update) | async-done | bytes 786448 | tf_op jit(solution)/shard_map/psum | solution.py:155
  295.5 2.6 copy.65
  298.1 7.1 %all-to-all-start.2 = ((bf16[16,12,2048]{2,1,0:T(8,128)(2,1)}), bf16[16,12,2048]{2,1,0:T(8,128)(2,1)}, u32[]{:S(2)}, u32[]{:S(2)}) async-start(bf16[16,12,2048]{2,1,0:T(8,128)(2,1)} %copy.65), calls=%async_computation.3 | async-start | bytes 2097152 | tf_op jit(solution)/shard_map/all_to_all | solution.py:157
  306.0 25.1 %all-to-all-done.2 = bf16[16,12,2048]{2,1,0:T(8,128)(2,1)} async-done(((bf16[16,12,2048]{2,1,0:T(8,128)(2,1)}), bf16[16,12,2048]{2,1,0:T(8,128)(2,1)}, u32[]{:S(2)}, u32[]{:S(2)}) %all-to-all-start.2) | async-done | bytes 786464 | tf_op jit(solution)/shard_map/all_to_all | solution.py:157
  331.1 2.1 reshape.169
  333.2 1.5 fusion.18
  (67 shorter events, 6.6 us)
Async XLA Ops:
  7.2 265.2 %copy-start = (bf16[1,704,2048]{2,1,0:T(8,128)(2,1)S(1)}, bf16[1,704,2048]{2,1,0:T(8,128)(2,1)}, u32[]{:S(2)}) copy-start(bf16[1,704,2048]{2,1,0:T(8,128)(2,1)} %param.39) | copy-start | bytes 8650756
  10.1 13.8 %all-to-all-start = ((bf16[32,16,128]{2,0,1:T(8,128)(2,1)}), bf16[32,16,128]{2,0,1:T(8,128)(2,1)S(1)}, u32[]{:S(2)}, u32[]{:S(2)}) async-start(bf16[32,16,128]{2,0,1:T(8,128)(2,1)} %copy_bitcast_fusion), calls=%async_computation | async-start | bytes 262144 | tf_op jit(solution)/shard_map/all_to_all | solution.py:82
  17.3 135.7 %reduce-scatter.2.cloned.1.call-start = ((), (), s32[]{:S(2)}) async-start(), calls=%async_computation.4 | async-start | bytes 2506752 | tf_op jit(solution)/shard_map/reduce_scatter | solution.py:84
  18.9 7.6 %copy-start.13 = (f32[32,4]{0,1:T(4,128)S(1)}, f32[32,4]{0,1:T(4,128)}, u32[]{:S(2)}) copy-start(f32[32,4]{0,1:T(4,128)} %param.35) | copy-start | bytes 1540
  18.9 7.7 %copy-start.7 = (s32[32,3]{0,1:T(4,128)S(1)}, s32[32,3]{0,1:T(4,128)}, u32[]{:S(2)}) copy-start(s32[32,3]{0,1:T(4,128)} %param.40) | copy-start | bytes 1156
  23.9 130.5 %copy-start.10 = (f32[4]{0:T(128)S(1)}, f32[4]{0:T(128)}, u32[]{:S(2)}) copy-start(f32[4]{0:T(128)} %param.30) | copy-start | bytes 52
  23.9 130.5 %copy-start.15 = (f32[4]{0:T(128)S(1)}, f32[4]{0:T(128)}, u32[]{:S(2)}) copy-start(f32[4]{0:T(128)} %param.29) | copy-start | bytes 52
  23.9 132.2 %copy-start.5 = (f32[32,4,64]{2,1,0:T(4,128)S(1)}, f32[32,4,64]{2,1,0:T(4,128)}, u32[]{:S(2)}) copy-start(f32[32,4,64]{2,1,0:T(4,128)} %param.34) | copy-start | bytes 98308
  25.8 179.9 %all-gather.2.cloned.1.call-start = ((), (), s32[]{:S(2)}) async-start(), calls=%async_computation.5 | async-start | bytes 1114112 | tf_op jit(solution)/shard_map/all_gather | solution.py:116
  26.5 200.0 %all-reduce.3.cloned.1.call-start = ((), (), s32[]{:S(2)}) async-start(), calls=%async_computation.6 | async-start | bytes 262144 | tf_op jit(solution)/shard_map/psum | solution.py:119
  27.3 180.6 %copy-start.11 = (s32[96]{0:T(128)}, s32[96]{0:T(128)S(1)}, u32[]{:S(2)}) copy-start(s32[96]{0:T(128)S(1)} %select_reduce_fusion) | copy-start | bytes 1156
  160.7 2.0 copy-start.1
  162.7 43.0 %copy-start.14 = (f32[256]{0:T(256)S(1)}, f32[256]{0:T(256)}, u32[]{:S(2)}) copy-start(f32[256]{0:T(256)} %param.31) | copy-start | bytes 3076
  162.7 63.8 %copy-start.2 = (bf16[32,2048]{1,0:T(8,128)(2,1)S(1)}, bf16[32,2048]{1,0:T(8,128)(2,1)}, u32[]{:S(2)}) copy-start(bf16[32,2048]{1,0:T(8,128)(2,1)} %param.21) | copy-start | bytes 393220
  162.7 64.9 %copy-start.6 = (f32[2048]{0:T(1024)S(1)}, f32[2048]{0:T(1024)}, u32[]{:S(2)}) copy-start(f32[2048]{0:T(1024)} %param.36) | copy-start | bytes 24580
  207.9 87.6 %all-reduce.5.cloned.1.call-start = ((), (), s32[]{:S(2)}) async-start(), calls=%async_computation.7 | async-start | bytes 1572864 | tf_op jit(solution)/shard_map/psum | solution.py:155
  267.5 1.0 copy-start.4
  277.5 27.7 %copy-start.12 = (s32[96]{0:T(128)S(1)}, s32[96]{0:T(128)}, u32[]{:S(2)}) copy-start(s32[96]{0:T(128)} %copy-done.11) | copy-start | bytes 1156
  277.5 27.8 %copy-start.8 = (s32[32,3]{0,1:T(4,128)S(1)}, s32[32,3]{0,1:T(4,128)}, u32[]{:S(2)}) copy-start(s32[32,3]{0,1:T(4,128)} %param.40) | copy-start | bytes 1156
  277.6 55.7 %copy-start.9 = (f32[32,3]{0,1:T(4,128)S(1)}, f32[32,3]{0,1:T(4,128)}, u32[]{:S(2)}) copy-start(f32[32,3]{0,1:T(4,128)} %param.41) | copy-start | bytes 1156
  298.1 36.6 %copy-start.3 = (bf16[32,2048]{1,0:T(8,128)(2,1)S(1)}, bf16[32,2048]{1,0:T(8,128)(2,1)}, u32[]{:S(2)}) copy-start(bf16[32,2048]{1,0:T(8,128)(2,1)} %all-reduce.3.cloned.1.call-done) | copy-start | bytes 393220
  298.1 33.0 %all-to-all-start.2 = ((bf16[16,12,2048]{2,1,0:T(8,128)(2,1)}), bf16[16,12,2048]{2,1,0:T(8,128)(2,1)}, u32[]{:S(2)}, u32[]{:S(2)}) async-start(bf16[16,12,2048]{2,1,0:T(8,128)(2,1)} %copy.65), calls=%async_computation.3 | async-start | bytes 2097152 | tf_op jit(solution)/shard_map/all_to_all | solution.py:157
Sparse Core Ops, SparseCore 0:
  25.9 127.0 reduce-scatter.1
  155.7 49.9 all-gather.1
  208.6 17.9 all-reduce.2
  277.7 17.7 all-reduce.4
where the time goes:
time: 343 us; the launch traced here: 342 us
  waiting for transfers between devices  230 us (67%)
  blocking collectives  33.1 us (10%)
  matrix products  20.2 us (6%)
  local copies, waits for them, and re-layouts  15.4 us (4%)
  starting transfers between devices  14.5 us (4%)
  other arithmetic  14.3 us (4%)
  between operations  14 us (4%)
    reduce_scatter x1, waiting for transfers between devices, body(): lax.psum_scatter(jnp.dot(spread, joined, preferred_element_type=jnp.float...  126 us
    all_gather x1, waiting for transfers between devices, body(): lax.all_gather(w_out, 'ep', axis=1, tiled=True)  39 us
    all_to_all x1, blocking collectives, body(): lax.all_to_all(outgoing, 'ep', split_axis=0, concat_axis=0, tiled=True)  33.1 us
    all_to_all x1, waiting for transfers between devices, body(): lax.all_to_all(finished, 'ep', split_axis=0, concat_axis=0, tiled=True)  25.1 us
    psum x1, waiting for transfers between devices, body(): lax.psum(partial_out.astype(jnp.bfloat16), 'tp').astype(jnp.float32)  18.1 us
    psum x1, waiting for transfers between devices, body(): expert_sum = lax.psum(partial_down.astype(jnp.bfloat16), 'tp')  17.9 us
    all_to_all x1, starting transfers between devices, body(): lax.all_to_all(normed, 'ep', split_axis=1, concat_axis=0, tiled=True)  7.22 us
    all_to_all x1, starting transfers between devices, body(): lax.all_to_all(finished, 'ep', split_axis=0, concat_axis=0, tiled=True)  7.11 us
  transfers between devices with their start and end apart: 6, of which 6 were waited for; matrix products, arithmetic and copies ran while one was open for 5% of the time, Pallas kernels for 0%

commit v1 on v0

--- a/solution.py
+++ b/solution.py
@@ -2,6 +2,29 @@
 import jax.numpy as jnp
 from jax import lax
 from jax.sharding import PartitionSpec as P
+from jax.lax import axis_index, axis_size, ppermute
+
+
+def turn_plane(matrix, d0):
+    matrix = jnp.moveaxis(matrix, 0, d0)
+    v_now = matrix.shape
+    big = matrix.reshape(*v_now[:d0], v_now[d0] * v_now[d0 + 1], *v_now[d0 + 2 :])
+    return big
+
+
+def deliver_sheets(array_in, peer_axis):
+    long_array = axis_size(peer_axis)
+    field_out = axis_index(peer_axis)
+    now, res = (long_array, field_out)
+    r1, next_value = (array_in[None], 1)
+    while next_value < now:
+        seen_now = ppermute(r1, peer_axis, [(nth, nth ^ next_value) for nth in range(now)])
+        answer = res & next_value == 0
+        formed = jnp.where(answer, r1, seen_now)
+        a_next = jnp.where(answer, seen_now, r1)
+        r1 = jnp.concatenate([formed, a_next])
+        next_value *= 2
+    return r1
 
 
 def rms_scale(values_in, gain_vec):
@@ -76,6 +99,12 @@
     routes,
     route_weights,
 ):
+
+    def _advance_turns(local_values, m, dim_i):
+        t_next = deliver_sheets(local_values, m)
+        reached = turn_plane(t_next, dim_i)
+        return reached
+
     seq_rows, width = tokens.shape
     normed = rms_scale(tokens, mix_gain).astype(jnp.bfloat16)
     weight_list = (w_query, w_key, w_value, w_outgate, w_igate, w_fgate)
@@ -112,9 +141,7 @@
         state_max,
     )
     partial_out = jnp.dot(
-        cell_out,
-        lax.all_gather(w_out, "ep", axis=1, tiled=True),
-        preferred_element_type=jnp.float32,
+        cell_out, _advance_turns(w_out, "ep", 1), preferred_element_type=jnp.float32
     )
     attended = lax.psum(partial_out.astype(jnp.bfloat16), "tp").astype(jnp.float32)
     resid = (tokens.astype(jnp.float32) + attended).astype(jnp.bfloat16)

time: 343 us -> 312 us (0.910)
  waiting for transfers between devices: 230 us -> 192 us
  other arithmetic: 14.3 us -> 19 us
    all_gather x1 -> x0, waiting for transfers between devices: 39 us -> none  [body(): lax.all_gather(w_out, 'ep', axis=1, tiled=True)]
    ppermute x0 -> x4, waiting for transfers between devices: none -> 38.4 us  [deliver_sheets(): ppermute(r1, peer_axis, [(nth, nth ^ next_value) for nth in range(now)])]
    reduce_scatter x1, waiting for transfers between devices: 126 us -> 89.6 us  [body(): lax.psum_scatter(jnp.dot(spread, joined, preferred_element_type=jnp.float...]
  transfers between devices with their start and end apart: 6 -> 9, of which waited for: 6 -> 9; matrix products, arithmetic and copies ran while one was open for 5% -> 3% of each run, Pallas kernels for 0% -> 0%
where the time goes in v1:
time: 312 us; the launch traced here: 311 us
  waiting for transfers between devices  192 us (62%)
  blocking collectives  33.1 us (11%)
  matrix products  20.4 us (7%)
  other arithmetic  19 us (6%)
  starting transfers between devices  16.8 us (5%)
  local copies, waits for them, and re-layouts  16.3 us (5%)
  between operations  14 us (4%)
    reduce_scatter x1, waiting for transfers between devices, body(): lax.psum_scatter(jnp.dot(spread, joined, preferred_element_type=jnp.float...  89.6 us
    ppermute x4, waiting for transfers between devices, deliver_sheets(): ppermute(r1, peer_axis, [(nth, nth ^ next_value) for nth in range(now)])  38.4 us
    all_to_all x1, blocking collectives, body(): lax.all_to_all(outgoing, 'ep', split_axis=0, concat_axis=0, tiled=True)  33.1 us
    all_to_all x1, waiting for transfers between devices, body(): lax.all_to_all(finished, 'ep', split_axis=0, concat_axis=0, tiled=True)  25.1 us
    psum x1, waiting for transfers between devices, body(): expert_sum = lax.psum(partial_down.astype(jnp.bfloat16), 'tp')  17.9 us
    psum x1, waiting for transfers between devices, body(): lax.psum(partial_out.astype(jnp.bfloat16), 'tp').astype(jnp.float32)  17 us
    all_to_all x1, starting transfers between devices, body(): lax.all_to_all(normed, 'ep', split_axis=1, concat_axis=0, tiled=True)  7.22 us
    all_to_all x1, starting transfers between devices, body(): lax.all_to_all(finished, 'ep', split_axis=0, concat_axis=0, tiled=True)  7.11 us
  transfers between devices with their start and end apart: 9, of which 9 were waited for; matrix products, arithmetic and copies ran while one was open for 3% of the time, Pallas kernels for 0%

profile of v1, /device:TPU:8, one launch (start us, length us, event | category | flops | bytes accessed | tf_op | source)
XLA Modules:
  0.0 311.4 jit_solution(2639817749791169274)
XLA Ops:
  7.2 1.2 fusion.36
  8.4 1.7 copy_bitcast_fusion
  10.1 7.2 %all-to-all-start = ((bf16[32,16,128]{2,0,1:T(8,128)(2,1)}), bf16[32,16,128]{2,0,1:T(8,128)(2,1)S(1)}, u32[]{:S(2)}, u32[]{:S(2)}) async-start(bf16[32,16,128]{2,0,1:T(8,128)(2,1)} %copy_bitcast_fusion), calls=%async_computation | async-start | bytes 262144 | tf_op jit(solution)/shard_map/all_to_all | solution.py:111
  18.9 1.1 concatenate.15
  20.0 3.9 %all-to-all-done = bf16[32,16,128]{2,0,1:T(8,128)(2,1)S(1)} async-done(((bf16[32,16,128]{2,0,1:T(8,128)(2,1)}), bf16[32,16,128]{2,0,1:T(8,128)(2,1)S(1)}, u32[]{:S(2)}, u32[]{:S(2)}) %all-to-all-start) | async-done | bytes 131104 | tf_op jit(solution)/shard_map/all_to_all | solution.py:111
  23.9 1.9 fusion.62
  26.6 3.7 %collective-permute-done = bf16[1,256,128]{1,2,0:T(8,128)(2,1)S(1)} collective-permute-done((bf16[1,256,128]{1,2,0:T(8,128)(2,1)S(1)}, bf16[1,256,128]{1,2,0:T(8,128)(2,1)S(1)}, u32[]{:S(2)}, u32[]{:S(2)}) %collective-permute-start) | collective-permute-done | bytes 65568 | tf_op jit(solution)/shard_map/ppermute | solution.py:21
  31.1 5.3 %collective-permute-done.1 = bf16[2,256,128]{1,2,0:T(8,128)(2,1)S(1)} collective-permute-done((bf16[2,256,128]{1,2,0:T(8,128)(2,1)S(1)}, bf16[2,256,128]{1,2,0:T(8,128)(2,1)S(1)}, u32[]{:S(2)}, u32[]{:S(2)}) %collective-permute-start.1) | collective-permute-done | bytes 131104 | tf_op jit(solution)/shard_map/ppermute | solution.py:21
  38.0 7.4 %collective-permute-done.2 = bf16[4,256,128]{1,2,0:T(8,128)(2,1)} collective-permute-done((bf16[4,256,128]{1,2,0:T(8,128)(2,1)S(1)}, bf16[4,256,128]{1,2,0:T(8,128)(2,1)}, u32[]{:S(2)}, u32[]{:S(2)}) %collective-permute-start.2) | collective-permute-done | bytes 262176 | tf_op jit(solution)/shard_map/ppermute | solution.py:21
  45.3 1.0 broadcast_select_fusion.3
  48.5 22.0 %collective-permute-done.3 = bf16[8,256,128]{1,2,0:T(8,128)(2,1)} collective-permute-done((bf16[8,256,128]{1,2,0:T(8,128)(2,1)}, bf16[8,256,128]{1,2,0:T(8,128)(2,1)}, u32[]{:S(2)}, u32[]{:S(2)}) %collective-permute-start.3) | collective-permute-done | bytes 524320 | tf_op jit(solution)/shard_map/ppermute | solution.py:21
  70.5 1.1 broadcast_select_fusion.1
  71.6 1.1 pad_maximum_fusion
  72.6 89.6 %reduce-scatter.2.cloned.1.call-done = f32[32,1032]{1,0:T(8,128)} async-done(((f32[512,1032]{1,0:T(8,128)}), f32[32,1032]{1,0:T(8,128)}) %reduce-scatter.2.cloned.1.call-update) | async-done | bytes 132112 | tf_op jit(solution)/shard_map/reduce_scatter | solution.py:113
  166.1 3.8 %multiply_add_fusion = f32[32,4,64,64]{3,2,1,0:T(8,128)S(1)} fusion(f32[32,4,64,64]{3,2,1,0:T(8,128)} %param.33, f32[32,4,64]{2,1,0:T(4,128)S(1)} %get-tuple-element.38, f32[32,4,64]{2,1,0:T(4,128)S(1)} %get-tuple-element.39, f32[32,4]{1,0:T(8,128)S(1)} %subtract_exponential_fusion.1), kind=kLoop, calls=%fused_computation | loop fusion | flops 1572864 | bytes 4260352 | tf_op jit(solution)/shard_map/add | solution.py:61
  169.9 2.0 copy-done.1
  172.0 3.4 %fusion.63 = f32[32,4,1,64]{3,2,1,0:T(1,128)S(1)} fusion(f32[32,4,64,64]{3,2,1,0:T(8,128)S(1)} %multiply_add_fusion, bf16[32,4,64,1]{2,3,1,0:T(2,128)(2,1)S(1)} %reshape.175), kind=kOutput, calls=%fused_computation.96 | convolution fusion | flops 6291456 | bytes 2146304 | tf_op jit(solution)/shard_map/bhvd,bhd->bhv/dot_general | solution.py:65
  176.0 2.3 convolution_convert_fusion.1
  179.0 17.0 %all-reduce.3.cloned.1.call-done = bf16[32,2048]{1,0:T(8,128)(2,1)} async-done(((bf16[32,2048]{1,0:T(8,128)(2,1)}), bf16[32,2048]{1,0:T(8,128)(2,1)}) %all-reduce.3.cloned.1.call-update) | async-done | bytes 131088 | tf_op jit(solution)/shard_map/psum | solution.py:146
  195.9 1.1 fusion.40
  198.2 1.1 reshape.157
  199.3 2.4 convolution_convert_fusion
  201.7 2.1 reshape.158
  203.9 33.1 %all_to_all.29 = bf16[16,12,2048]{2,1,0:T(8,128)(2,1)S(1)} all-to-all(bf16[16,12,2048]{2,1,0:T(8,128)(2,1)} %reshape.158), channel_id=1, replica_groups=mesh['ep'=16,'tp'=2] {'ep'}, dimensions={0} | all-to-all | bytes 1572864 | tf_op jit(solution)/shard_map/all_to_all | solution.py:169
  237.9 3.8 %fusion.9 = f32[16,1,12,704]{3,0,2,1:T(8,128)} fusion(bf16[1,2048,704]{1,2,0:T(8,128)(2,1)} %param.37, bf16[16,12,2048]{2,1,0:T(8,128)(2,1)S(1)} %all_to_all.29), kind=kOutput, calls=%fused_computation.11 | convolution fusion | flops 553648128 | bytes 4210688 | tf_op jit(solution)/shard_map/nxcd,xdf->nxcf/dot_general | solution.py:172
  241.7 5.2 %fusion.6 = bf16[16,12,2048]{2,0,1:T(8,128)(2,1)} fusion(bf16[1,704,2048]{2,1,0:T(8,128)(2,1)S(1)} %copy-done, bf16[1,2048,704]{1,2,0:T(8,128)(2,1)} %param.38, f32[16,1,12,704]{3,0,2,1:T(8,128)} %fusion.9, bf16[16,12,2048]{2,1,0:T(8,128)(2,1)} %copy-done.5), kind=kOutput, calls=%fused_computation.7 | convolution fusion | flops 1108500480 | bytes 7880704 | tf_op jit(solution)/shard_map/nxcf,xfd->nxcd/dot_general | solution.py:179
  247.0 17.9 %all-reduce.5.cloned.1.call-done = bf16[16,12,2048]{2,0,1:T(8,128)(2,1)} async-done(((bf16[16,12,2048]{2,0,1:T(8,128)(2,1)}), bf16[16,12,2048]{2,0,1:T(8,128)(2,1)}) %all-reduce.5.cloned.1.call-update) | async-done | bytes 786448 | tf_op jit(solution)/shard_map/psum | solution.py:182
  264.9 2.6 copy.68
  267.5 7.1 %all-to-all-start.2 = ((bf16[16,12,2048]{2,1,0:T(8,128)(2,1)}), bf16[16,12,2048]{2,1,0:T(8,128)(2,1)}, u32[]{:S(2)}, u32[]{:S(2)}) async-start(bf16[16,12,2048]{2,1,0:T(8,128)(2,1)} %copy.68), calls=%async_computation.3 | async-start | bytes 2097152 | tf_op jit(solution)/shard_map/all_to_all | solution.py:184
  275.5 25.1 %all-to-all-done.2 = bf16[16,12,2048]{2,1,0:T(8,128)(2,1)} async-done(((bf16[16,12,2048]{2,1,0:T(8,128)(2,1)}), bf16[16,12,2048]{2,1,0:T(8,128)(2,1)}, u32[]{:S(2)}, u32[]{:S(2)}) %all-to-all-start.2) | async-done | bytes 786464 | tf_op jit(solution)/shard_map/all_to_all | solution.py:184
  300.6 2.2 reshape.173
  302.7 1.5 fusion.18
  (85 shorter events, 15.8 us)
Async XLA Ops:
  7.2 234.6 %copy-start = (bf16[1,704,2048]{2,1,0:T(8,128)(2,1)S(1)}, bf16[1,704,2048]{2,1,0:T(8,128)(2,1)}, u32[]{:S(2)}) copy-start(bf16[1,704,2048]{2,1,0:T(8,128)(2,1)} %param.39) | copy-start | bytes 8650756
  10.1 13.8 %all-to-all-start = ((bf16[32,16,128]{2,0,1:T(8,128)(2,1)}), bf16[32,16,128]{2,0,1:T(8,128)(2,1)S(1)}, u32[]{:S(2)}, u32[]{:S(2)}) async-start(bf16[32,16,128]{2,0,1:T(8,128)(2,1)} %copy_bitcast_fusion), calls=%async_computation | async-start | bytes 262144 | tf_op jit(solution)/shard_map/all_to_all | solution.py:111
  17.3 145.0 %reduce-scatter.2.cloned.1.call-start = ((), (), s32[]{:S(2)}) async-start(), calls=%async_computation.4 | async-start | bytes 2506752 | tf_op jit(solution)/shard_map/reduce_scatter | solution.py:113
  18.9 6.9 %copy-start.7 = (bf16[256,128]{1,0:T(8,128)(2,1)S(1)}, bf16[256,128]{1,0:T(8,128)(2,1)}, u32[]{:S(2)}) copy-start(bf16[256,128]{1,0:T(8,128)(2,1)} %param.32) | copy-start | bytes 196612
  25.7 21.5 %copy-start.16 = (f32[32,4]{0,1:T(4,128)S(1)}, f32[32,4]{0,1:T(4,128)}, u32[]{:S(2)}) copy-start(f32[32,4]{0,1:T(4,128)} %param.35) | copy-start | bytes 1540
  25.7 21.6 %copy-start.9 = (s32[32,3]{0,1:T(4,128)S(1)}, s32[32,3]{0,1:T(4,128)}, u32[]{:S(2)}) copy-start(s32[32,3]{0,1:T(4,128)} %param.40) | copy-start | bytes 1156
  25.8 170.1 %all-reduce.3.cloned.1.call-start = ((), (), s32[]{:S(2)}) async-start(), calls=%async_computation.5 | async-start | bytes 262144 | tf_op jit(solution)/shard_map/psum | solution.py:146
  25.9 4.3 %collective-permute-start = (bf16[1,256,128]{1,2,0:T(8,128)(2,1)S(1)}, bf16[1,256,128]{1,2,0:T(8,128)(2,1)S(1)}, u32[]{:S(2)}, u32[]{:S(2)}) collective-permute-start(bf16[1,256,128]{1,2,0:T(8,128)(2,1)S(1)} %bitcast.79), channel_id=1, source_target_pairs={{0,2},{2,0},{4,6},{6,4},{8,10},{10,8},{12,14},{14,12},{16,18},{18,... | collective-permute-start | bytes 196616 | tf_op jit(solution)/shard_map/ppermute | solution.py:21
  30.3 6.1 %collective-permute-start.1 = (bf16[2,256,128]{1,2,0:T(8,128)(2,1)S(1)}, bf16[2,256,128]{1,2,0:T(8,128)(2,1)S(1)}, u32[]{:S(2)}, u32[]{:S(2)}) collective-permute-start(bf16[2,256,128]{1,2,0:T(8,128)(2,1)S(1)} %pad_maximum_fusion.3), channel_id=1, source_target_pairs={{0,4},{2,6},{4,0},{6,2},{8,12},{10,14},{12,8},{14,10},{16,20},{18,... | collective-permute-start | bytes 393224 | tf_op jit(solution)/shard_map/ppermute | solution.py:21
  36.4 0.7 copy-start.4
  37.1 8.2 %collective-permute-start.2 = (bf16[4,256,128]{1,2,0:T(8,128)(2,1)S(1)}, bf16[4,256,128]{1,2,0:T(8,128)(2,1)}, u32[]{:S(2)}, u32[]{:S(2)}) collective-permute-start(bf16[4,256,128]{1,2,0:T(8,128)(2,1)S(1)} %pad_maximum_fusion.2), channel_id=1, source_target_pairs={{0,8},{2,10},{4,12},{6,14},{8,0},{10,2},{12,4},{14,6},{16,24},{18,... | collective-permute-start | bytes 786440 | tf_op jit(solution)/shard_map/ppermute | solution.py:21
  47.2 23.2 %collective-permute-start.3 = (bf16[8,256,128]{1,2,0:T(8,128)(2,1)}, bf16[8,256,128]{1,2,0:T(8,128)(2,1)}, u32[]{:S(2)}, u32[]{:S(2)}) collective-permute-start(bf16[8,256,128]{1,2,0:T(8,128)(2,1)} %pad_maximum_fusion.1), channel_id=1, source_target_pairs={{0,16},{2,18},{4,20},{6,22},{8,24},{10,26},{12,28},{14,30},{16,0},... | collective-permute-start | bytes 1572872 | tf_op jit(solution)/shard_map/ppermute | solution.py:21
  47.5 116.0 %copy-start.11 = (s32[96]{0:T(128)}, s32[96]{0:T(128)S(1)}, u32[]{:S(2)}) copy-start(s32[96]{0:T(128)S(1)} %eq.66) | copy-start | bytes 1156
  48.5 116.9 %copy-start.6 = (f32[32,4,64]{2,1,0:T(4,128)S(1)}, f32[32,4,64]{2,1,0:T(4,128)}, u32[]{:S(2)}) copy-start(f32[32,4,64]{2,1,0:T(4,128)} %param.34) | copy-start | bytes 98308
  169.9 2.0 copy-start.1
  171.9 4.0 %copy-start.17 = (f32[256]{0:T(256)S(1)}, f32[256]{0:T(256)}, u32[]{:S(2)}) copy-start(f32[256]{0:T(256)} %param.31) | copy-start | bytes 3076
  171.9 6.4 %copy-start.12 = (s32[96]{0:T(128)S(1)}, s32[96]{0:T(128)}, u32[]{:S(2)}) copy-start(s32[96]{0:T(128)} %copy-done.11) | copy-start | bytes 1156
  171.9 6.4 %copy-start.14 = (s32[96]{0:T(128)S(1)}, s32[96]{0:T(128)}, u32[]{:S(2)}) copy-start(s32[96]{0:T(128)} %select_reduce_fusion) | copy-start | bytes 1156
  171.9 24.0 %copy-start.2 = (bf16[32,2048]{1,0:T(8,128)(2,1)S(1)}, bf16[32,2048]{1,0:T(8,128)(2,1)}, u32[]{:S(2)}) copy-start(bf16[32,2048]{1,0:T(8,128)(2,1)} %param.21) | copy-start | bytes 393220
  171.9 25.0 %copy-start.8 = (f32[2048]{0:T(1024)S(1)}, f32[2048]{0:T(1024)}, u32[]{:S(2)}) copy-start(f32[2048]{0:T(1024)} %param.36) | copy-start | bytes 24580
  178.3 86.6 %all-reduce.5.cloned.1.call-start = ((), (), s32[]{:S(2)}) async-start(), calls=%async_computation.6 | async-start | bytes 1572864 | tf_op jit(solution)/shard_map/psum | solution.py:182
  237.0 1.0 copy-start.5
  247.0 27.7 %copy-start.15 = (s32[96]{0:T(128)S(1)}, s32[96]{0:T(128)}, u32[]{:S(2)}) copy-start(s32[96]{0:T(128)} %select_reduce_fusion) | copy-start | bytes 1156
  247.0 27.8 %copy-start.10 = (s32[32,3]{0,1:T(4,128)S(1)}, s32[32,3]{0,1:T(4,128)}, u32[]{:S(2)}) copy-start(s32[32,3]{0,1:T(4,128)} %param.40) | copy-start | bytes 1156
  247.0 55.7 %copy-start.13 = (f32[32,3]{0,1:T(4,128)S(1)}, f32[32,3]{0,1:T(4,128)}, u32[]{:S(2)}) copy-start(f32[32,3]{0,1:T(4,128)} %param.41) | copy-start | bytes 1156
  267.5 36.7 %copy-start.3 = (bf16[32,2048]{1,0:T(8,128)(2,1)S(1)}, bf16[32,2048]{1,0:T(8,128)(2,1)}, u32[]{:S(2)}) copy-start(bf16[32,2048]{1,0:T(8,128)(2,1)} %all-reduce.3.cloned.1.call-done) | copy-start | bytes 393220
  267.5 33.0 %all-to-all-start.2 = ((bf16[16,12,2048]{2,1,0:T(8,128)(2,1)}), bf16[16,12,2048]{2,1,0:T(8,128)(2,1)}, u32[]{:S(2)}, u32[]{:S(2)}) async-start(bf16[16,12,2048]{2,1,0:T(8,128)(2,1)} %copy.68), calls=%async_computation.3 | async-start | bytes 2097152 | tf_op jit(solution)/shard_map/all_to_all | solution.py:184
Sparse Core Ops, SparseCore 0:
  25.9 136.3 reduce-scatter.1
  178.4 17.4 all-reduce.2
  247.1 17.7 all-reduce.4
